TPU v7x, 32 devices: a whole 2x2x4 slice. The times are simulated.
32 devices in a mesh: grp: 2 (over x), kv: 4 (over z), tp: 4 (over y, core).
Axes of the slice: x: 2, y: 2, z: 4, core: 2. Of those that a mesh axis runs over, the one named last changes fastest.
Arguments:
- tokens: bfloat16 [16, 4096], P('grp', 'tp'), parts along dimension 0, may hold values from -50 to 50
- pre_gain: float32 [4096], P('tp'), may hold values from 0.1 to 1.9
- gate_first: bfloat16 [4096, 11264], P('tp', 'kv'), may hold values from -0.09375 to 0.09375
- up_first: bfloat16 [4096, 11264], P('tp', 'kv'), may hold values from -0.09375 to 0.09375
- down_first: bfloat16 [11264, 4096], P('kv', 'tp'), may hold values from -0.0546875 to 0.0546875
- mix_gain: float32 [4096], P('tp'), may hold values from 0.1 to 1.9
- query_w: bfloat16 [4096, 4096], P('tp', 'kv'), may hold values from -0.09375 to 0.09375
- key_w: bfloat16 [4096, 4096], P('tp', 'kv'), may hold values from -0.09375 to 0.09375
- value_w: bfloat16 [4096, 4096], P('tp', 'kv'), may hold values from -0.09375 to 0.09375
- forget_w: bfloat16 [4096, 32], P('tp'), may hold values from -0.09375 to 0.09375
- key_cache: bfloat16 [16, 1024, 4096], P('grp', 'tp', 'kv'), parts along dimension 0, may hold values from -800 to 800
- value_cache: bfloat16 [16, 1024, 4096], P('grp', 'tp', 'kv'), parts along dimension 0, may hold values from -6 to 6
- gate_cache: float32 [16, 32, 1024], P('grp', 'kv', 'tp'), parts along dimension 0, may hold values from -130 to 0, as said below
- lengths: int32 [16], P('grp'), parts along dimension 0, may hold values from 64 to 1024, as said below
- out_w: bfloat16 [4096, 4096], P('kv', 'tp'), may hold values from -0.09375 to 0.09375
- post_gain: float32 [4096], P('tp'), may hold values from 0.1 to 1.9
- gate_second: bfloat16 [4096, 11264], P('tp', 'kv'), may hold values from -0.09375 to 0.09375
- up_second: bfloat16 [4096, 11264], P('tp', 'kv'), may hold values from -0.09375 to 0.09375
- down_second: bfloat16 [11264, 4096], P('kv', 'tp'), may hold values from -0.0546875 to 0.0546875
Outputs:
- out: bfloat16 [16, 4096], P('grp', 'tp'), parts along dimension 0
There are 2 independent parts, one for each index of `grp`. A program takes and returns all parts, laid end to end along the dimension named above; an argument that names none is the same for every part. Nothing has to cross between parts.
Inputs may be any that keep to these rules, and one draw needn't show every extreme that they name: `lengths`: each sequence's count of live cache positions; one sequence has all 1024 in every draw. `gate_cache`: at a live position p of sequence b, the sum of the log forget values of positions p + 1 to lengths[b] - 1 (zero at the last live position); never positive; zero beyond the live positions.
All inputs are finite; a program needn't handle non-finite values.
Results may differ from a plain program's by a relative error of at most 0.015.
Values may be sent and summed in bfloat16 or wider, within the bound.
A program may use at most 128 MiB of HBM per device.

v0:
```python
import jax
import jax.numpy as jnp
from jax import lax
from jax.sharding import PartitionSpec as P

D = 4096
HEAD_DIM = 128


EPSILON = 1e-06
MASKED = -1e30


def half_step(tok_rows, gain_part, w_gate, w_up, w_down):
    widened = tok_rows.astype(jnp.float32)
    squares = jnp.sum(widened * widened, axis=1)
    weighted = (widened * gain_part).astype(jnp.bfloat16)
    gate_part = jnp.dot(weighted, w_gate, preferred_element_type=jnp.float32)
    up_part = jnp.dot(weighted, w_up, preferred_element_type=jnp.float32)
    gate_sum, up_sum, sq_total = (
        lax.psum(gate_part.astype(jnp.bfloat16), "tp").astype(jnp.float32),
        lax.psum(up_part.astype(jnp.bfloat16), "tp").astype(jnp.float32),
        lax.psum(squares.astype(jnp.bfloat16), "tp").astype(jnp.float32),
    )
    norm_scale = lax.rsqrt(sq_total / D + EPSILON)[:, None]
    hidden = (jax.nn.silu(norm_scale * gate_sum) * (norm_scale * up_sum)).astype(jnp.bfloat16)
    down_part = jnp.dot(hidden, w_down, preferred_element_type=jnp.float32)
    down_sum = lax.psum(down_part, "kv")
    return (widened + 0.5 * down_sum).astype(jnp.bfloat16)


def absorb_parts(running, shard_part):
    run_top, run_mass, run_sum = running
    piece_top, masses, piece_sum = shard_part
    new_top = jnp.maximum(run_top, jnp.max(piece_top, axis=0))
    rescale = jnp.exp(run_top - new_top)
    factors = jnp.exp(piece_top - new_top[None])
    run_mass = run_mass * rescale + jnp.sum(masses * factors, axis=0)
    run_sum = run_sum * rescale[:, :, None] + jnp.sum(
        piece_sum.astype(jnp.float32) * factors[:, :, :, None], axis=0
    )
    return (new_top, run_mass, run_sum)


def attention(
    tok_rows,
    mix_gain,
    query_w,
    key_w,
    value_w,
    forget_w,
    key_cache,
    value_cache,
    gate_cache,
    lengths,
):
    widened = tok_rows.astype(jnp.float32)
    squares = jnp.sum(widened * widened, axis=1)
    weighted = (widened * mix_gain).astype(jnp.bfloat16)
    query_part = jnp.dot(weighted, query_w, preferred_element_type=jnp.float32)
    key_part = jnp.dot(weighted, key_w, preferred_element_type=jnp.float32)
    value_part = jnp.dot(weighted, value_w, preferred_element_type=jnp.float32)
    forget_part = jnp.dot(weighted, forget_w, preferred_element_type=jnp.float32)
    query_sum, key_sum, value_sum, forget_sum, sq_total = lax.psum(
        (query_part, key_part, value_part, forget_part, squares), "tp"
    )
    norm_scale = lax.rsqrt(sq_total / D + EPSILON)[:, None]
    query = (norm_scale * query_sum).astype(jnp.bfloat16)
    key_new = (norm_scale * key_sum).astype(jnp.bfloat16)
    value_new = (norm_scale * value_sum).astype(jnp.bfloat16)
    batch_rows = tok_rows.shape[0]
    heads_here = query.shape[1] // HEAD_DIM
    head_start = lax.axis_index("kv") * heads_here
    log_forget = jax.nn.log_sigmoid(
        norm_scale * lax.dynamic_slice_in_dim(forget_sum, head_start, heads_here, 1)
    )
    cache_span = key_cache.shape[1]
    query_heads = query.reshape(batch_rows, heads_here, HEAD_DIM)
    key_block = key_cache.reshape(batch_rows, cache_span, heads_here, HEAD_DIM)
    value_block = value_cache.reshape(batch_rows, cache_span, heads_here, HEAD_DIM)
    scores = jnp.einsum(
        "bhd,bphd->bhp", query_heads, key_block, preferred_element_type=jnp.float32
    ) * HEAD_DIM ** (-0.5)
    scores = scores + gate_cache + log_forget[:, :, None]
    slot_positions = lax.axis_index("tp") * cache_span + lax.iota(jnp.int32, cache_span)
    is_live = slot_positions[None, None, :] < lengths[:, None, None]
    local_top = jnp.max(jnp.where(is_live, scores, MASKED), axis=2)
    local_probs = jnp.where(is_live, jnp.exp(scores - local_top[:, :, None]), 0.0)
    local_mass = jnp.sum(local_probs, axis=2)
    local_sum = jnp.einsum(
        "bhp,bphd->bhd",
        local_probs.astype(jnp.bfloat16),
        value_block,
        preferred_element_type=jnp.float32,
    ).astype(jnp.bfloat16)
    initial = (
        jnp.full((batch_rows, heads_here), MASKED, jnp.float32),
        jnp.zeros((batch_rows, heads_here), jnp.float32),
        jnp.zeros((batch_rows, heads_here, HEAD_DIM), jnp.float32),
    )
    run_top, run_mass, run_sum = absorb_parts(
        initial,
        (
            lax.all_gather(local_top[None].astype(jnp.bfloat16), "tp", axis=0, tiled=True).astype(
                jnp.float32
            ),
            lax.all_gather(local_mass[None].astype(jnp.bfloat16), "tp", axis=0, tiled=True).astype(
                jnp.float32
            ),
            lax.all_gather(local_sum[None], "tp", axis=0, tiled=True),
        ),
    )
    new_heads = key_new.reshape(batch_rows, heads_here, HEAD_DIM).astype(jnp.float32)
    own_score = jnp.sum(query_heads.astype(jnp.float32) * new_heads, axis=2) * HEAD_DIM ** (-0.5)
    highest = jnp.maximum(run_top, own_score)
    rescale = jnp.exp(run_top - highest)
    own_weight = jnp.exp(own_score - highest)
    own_values = value_new.reshape(batch_rows, heads_here, HEAD_DIM).astype(jnp.float32)
    numer = run_sum * rescale[:, :, None] + own_weight[:, :, None] * own_values
    denom = run_mass * rescale + own_weight
    return (
        (numer / denom[:, :, None]).astype(jnp.bfloat16).reshape(batch_rows, heads_here * HEAD_DIM)
    )


def on_device(
    tokens,
    pre_gain,
    gate_first,
    up_first,
    down_first,
    mix_gain,
    query_w,
    key_w,
    value_w,
    forget_w,
    key_cache,
    value_cache,
    gate_cache,
    lengths,
    out_w,
    post_gain,
    gate_second,
    up_second,
    down_second,
):
    after_first = half_step(tokens, pre_gain, gate_first, up_first, down_first)
    attended = attention(
        after_first,
        mix_gain,
        query_w,
        key_w,
        value_w,
        forget_w,
        key_cache,
        value_cache,
        gate_cache,
        lengths,
    )
    projected = lax.psum(jnp.dot(attended, out_w, preferred_element_type=jnp.float32), "kv")
    residual_two = (after_first.astype(jnp.float32) + projected).astype(jnp.bfloat16)
    return half_step(residual_two, post_gain, gate_second, up_second, down_second)


def solution(mesh):
    placed = (
        P("grp", "tp"),
        P("tp"),
        P("tp", "kv"),
        P("tp", "kv"),
        P("kv", "tp"),
        P("tp"),
        P("tp", "kv"),
        P("tp", "kv"),
        P("tp", "kv"),
        P("tp", None),
        P("grp", "tp", "kv"),
        P("grp", "tp", "kv"),
        P("grp", "kv", "tp"),
        P("grp"),
        P("kv", "tp"),
        P("tp"),
        P("tp", "kv"),
        P("tp", "kv"),
        P("kv", "tp"),
    )
    return jax.shard_map(
        on_device, mesh=mesh, in_specs=placed, out_specs=P("grp", "tp"), check_vma=False
    )
```

profile of v0, /device:TPU:0, one launch (start us, length us, event | category | flops | bytes accessed | tf_op | source)
XLA Modules:
  0.0 220.3 jit_solution(18089456365356496139)
XLA Ops:
  6.5 0.0 copy-start
  6.5 0.0 copy-start.4
  6.5 0.0 copy-start.9
  6.5 0.0 all-reduce.11.cloned.1.call-start
  6.5 0.0 copy-start.1
  6.6 1.5 fusion.15
  8.1 4.5 %convolution_convert_fusion.3 = bf16[8,2816]{1,0:T(8,128)(2,1)} fusion(bf16[1024,2816]{1,0:T(8,128)(2,1)} %param.21, bf16[8,1024]{1,0:T(8,128)(2,1)} %param.19, f32[1024]{0:T(1024)} %param.20), kind=kOutput, calls=%fused_computation.6 | convolution fusion | flops 46184448 | bytes 5832704 | tf_op jit(solution)/shard_map/dot_general | solution.py:18
  12.6 0.0 copy-done.4
  12.6 0.0 copy-done.9
  12.6 0.0 copy-done.1
  12.6 1.5 convolution_convert_fusion.2
  14.1 0.0 all-reduce.11.cloned.1.call-update
  14.1 0.0 all-reduce.7.cloned.1.call-start
  14.1 33.9 %all-reduce.11.cloned.1.call-done = (bf16[8,2816]{1,0:T(8,128)(2,1)}, bf16[8,2816]{1,0:T(8,128)(2,1)}, bf16[8]{0:T(256)(128)(2,1)}) async-done(((bf16[8,2816]{1,0:T(8,128)(2,1)}, bf16[8,2816]{1,0:T(8,128)(2,1)}, bf16[8]{0:T(256)(128)(2,1)}), (bf16[8,2816]{1,0:T(8,128)(2,1)}, bf16[8,2816]{1,0:T(8,128)(2,1)}, bf16[8]{0:T(256)(128)(2,1)})) %all-reduce.11.cloned.1.call-update) | async-done | bytes 90144 | tf_op jit(solution)/shard_map/psum | solution.py:22
  48.1 0.7 add_rsqrt_fusion.2
  48.7 3.6 %fusion.9 = f32[8,1024]{1,0:T(8,128)S(1)} fusion(bf16[2816,1024]{1,0:T(8,128)(2,1)} %param.23, bf16[8,2816]{1,0:T(8,128)(2,1)} %get-tuple-element.13, bf16[8,2816]{1,0:T(8,128)(2,1)} %get-tuple-element.14, f32[8]{0:T(128)S(1)} %add_rsqrt_fusion.2), kind=kOutput, calls=%fused_computation.28 | convolution fusion | flops 46362624 | bytes 5890080 | tf_op jit(solution)/shard_map/dot_general | solution.py:27
  52.3 19.1 %psum.101 = f32[8,1024]{1,0:T(8,128)S(1)} all-reduce(f32[8,1024]{1,0:T(8,128)S(1)} %fusion.9), channel_id=1, replica_groups=mesh['grp'=2,'kv'=4,'tp'=4] {'kv'}, use_global_device_ids=true, to_apply=%region_4.5 | all-reduce | flops 8192 | bytes 65536 | tf_op jit(solution)/shard_map/psum | solution.py:28
  71.4 0.0 copy-start.3
  71.4 0.7 fusion.18
  72.1 0.0 copy-done.5
  72.1 0.0 copy-done.7
  72.2 0.7 fusion.45
  72.9 0.0 copy-done
  72.9 1.0 fusion.43
  73.9 2.6 %fusion.41 = f32[8,1024]{1,0:T(8,128)} fusion(bf16[1024,1024]{1,0:T(8,128)(2,1)} %param.27, bf16[8,1024]{1,0:T(8,128)(2,1)S(1)} %get-tuple-element.21, f32[1024]{0:T(1024)S(1)} %copy-done.5), kind=kOutput, calls=%fused_computation.68 | convolution fusion | flops 16801792 | bytes 2150400 | tf_op jit(solution)/shard_map/dot_general | solution.py:62
  76.4 0.0 copy-done.3
  76.4 1.0 fusion.47
  77.4 0.0 all-reduce.7.cloned.1.call-update
  77.5 0.0 all-reduce.9.cloned.1.call-start
  77.5 0.0 copy-done.11
  77.5 0.1 broadcast_compare_fusion
  77.6 6.4 %copy.38 = bf16[8,256,1024]{1,2,0:T(8,128)(2,1)} copy(bf16[8,256,1024]{2,1,0:T(8,128)(2,1)} %param.29) | data formatting | bytes 8388608 | tf_op jit(solution)/shard_map/reshape | solution.py:79
  84.0 21.8 %all-reduce.7.cloned.1.call-done = (f32[8,1024]{1,0:T(8,128)}, f32[8]{0:T(128)}, f32[8,32]{1,0:T(8,128)}, f32[8,1024]{1,0:T(8,128)}, f32[8,1024]{1,0:T(8,128)}) async-done(((f32[8,1024]{1,0:T(8,128)}, f32[8]{0:T(128)}, f32[8,32]{1,0:T(8,128)}, f32[8,1024]{1,0:T(8,128)}, f32[8,1024]{1,0:T(8,128)}), (f32[8,1024]{1,0:T(8,128)}, f32[8]{0:T(128)}, f32[8,32]{1,0:T(8,128)}, f32[8,1024]{1,0:T(8,128)}, ...) | async-done | bytes 99376 | tf_op jit(solution)/shard_map/psum | solution.py:64
  105.8 0.7 add_rsqrt_fusion.1
  106.5 0.8 fusion.54
  107.4 0.9 fusion.27
  108.3 0.1 copy.29
  108.4 0.8 fusion.51
  109.1 2.8 %fusion.28 = f32[8,8,1,256]{3,2,1,0:T(1,128)S(1)} fusion(bf16[8,256,8,128]{1,3,2,0:T(8,128)(2,1)} %bitcast.68, bf16[8,8,128,1]{2,0,1,3:T(8,128)(2,1)S(1)} %fusion.54), kind=kOutput, calls=%fused_computation.50 | convolution fusion | flops 4194304 | bytes 4276224 | tf_op jit(solution)/shard_map/bhd,bphd->bhp/dot_general | solution.py:81
  112.0 0.0 copy-done.6
  112.0 0.2 select_reduce_fusion
  112.2 0.2 fusion.7
  112.3 5.2 %all-gather = bf16[32,8]{1,0:T(8,128)(2,1)S(1)} all-gather(bf16[8,8]{1,0:T(8,128)(2,1)S(1)} %convert_element_type.152), channel_id=2, replica_groups=mesh['grp'=2,'kv'=4,'tp'=4] {'tp'}, dimensions={0}, use_global_device_ids=true | all-gather | bytes 640 | tf_op jit(solution)/shard_map/all_gather | solution.py:104
  117.6 5.5 %all-gather.2 = bf16[32,8]{1,0:T(8,128)(2,1)S(1)} all-gather(bf16[8,8]{1,0:T(8,128)(2,1)S(1)} %get-tuple-element.22), channel_id=4, replica_groups=mesh['grp'=2,'kv'=4,'tp'=4] {'tp'}, dimensions={0}, use_global_device_ids=true | all-gather | bytes 640 | tf_op jit(solution)/shard_map/all_gather | solution.py:107
  123.1 0.1 copy.30
  123.2 0.1 copy.31
  123.2 3.0 %fusion = f32[8,8,1,128]{3,2,1,0:T(1,128)S(1)} fusion(bf16[8,8,256,1]{2,1,0,3:T(8,128)(2,1)S(1)} %get-tuple-element.23, bf16[8,256,1024]{2,1,0:T(8,128)(2,1)} %param.30), kind=kOutput, calls=%fused_computation | convolution fusion | flops 4194304 | bytes 4259840 | tf_op jit(solution)/shard_map/bhp,bphd->bhd/dot_general | solution.py:90
  126.2 5.2 %all-gather.1 = bf16[32,8,128]{2,1,0:T(8,128)(2,1)S(1)} all-gather(bf16[8,8,128]{2,1,0:T(8,128)(2,1)S(1)} %convert_element_type.155), channel_id=3, replica_groups=mesh['grp'=2,'kv'=4,'tp'=4] {'tp'}, dimensions={0}, use_global_device_ids=true | all-gather | bytes 81920 | tf_op jit(solution)/shard_map/all_gather | solution.py:110
  131.5 0.1 fusion.3
  131.6 0.1 multiply_bitcast_fusion
  131.6 0.0 copy-done.8
  131.7 0.0 copy-done.2
  131.7 0.4 fusion.31
  132.1 19.3 %psum.107 = f32[8,1024]{1,0:T(8,128)S(1)} all-reduce(f32[8,1024]{1,0:T(8,128)S(1)} %fusion.31), channel_id=1, replica_groups=mesh['grp'=2,'kv'=4,'tp'=4] {'kv'}, use_global_device_ids=true, to_apply=%region_17.18 | all-reduce | flops 8192 | bytes 65536 | tf_op jit(solution)/shard_map/psum | solution.py:160
  151.4 0.6 fusion.21
  152.1 0.0 copy-done.10
  152.1 4.1 %convolution_convert_fusion.1 = bf16[8,2816]{1,0:T(8,128)(2,1)} fusion(bf16[1024,2816]{1,0:T(8,128)(2,1)} %param.35, bf16[8,1024]{1,0:T(8,128)(2,1)S(1)} %get-tuple-element.17, f32[1024]{0:T(1024)S(1)} %copy-done.10), kind=kOutput, calls=%fused_computation.4 | convolution fusion | flops 46184448 | bytes 5832704 | tf_op jit(solution)/shard_map/dot_general | solution.py:18
  156.2 4.1 %convolution_convert_fusion = bf16[8,2816]{1,0:T(8,128)(2,1)} fusion(bf16[1024,2816]{1,0:T(8,128)(2,1)} %param.36, bf16[8,1024]{1,0:T(8,128)(2,1)S(1)} %get-tuple-element.17, f32[1024]{0:T(1024)S(1)} %copy-done.10), kind=kOutput, calls=%fused_computation.3 | convolution fusion | flops 46184448 | bytes 5832704 | tf_op jit(solution)/shard_map/dot_general | solution.py:19
  160.3 0.0 all-reduce.9.cloned.1.call-update
  160.3 29.6 %all-reduce.9.cloned.1.call-done = (bf16[8,2816]{1,0:T(8,128)(2,1)}, bf16[8,2816]{1,0:T(8,128)(2,1)}, bf16[8]{0:T(256)(128)(2,1)}) async-done(((bf16[8,2816]{1,0:T(8,128)(2,1)}, bf16[8,2816]{1,0:T(8,128)(2,1)}, bf16[8]{0:T(256)(128)(2,1)}), (bf16[8,2816]{1,0:T(8,128)(2,1)}, bf16[8,2816]{1,0:T(8,128)(2,1)}, bf16[8]{0:T(256)(128)(2,1)})) %all-reduce.9.cloned.1.call-update) | async-done | bytes 90144 | tf_op jit(solution)/shard_map/psum | solution.py:22
  190.0 0.7 add_rsqrt_fusion
  190.6 3.6 %fusion.10 = f32[8,1024]{1,0:T(8,128)S(1)} fusion(bf16[2816,1024]{1,0:T(8,128)(2,1)} %param.37, bf16[8,2816]{1,0:T(8,128)(2,1)} %get-tuple-element.10, bf16[8,2816]{1,0:T(8,128)(2,1)} %get-tuple-element.11, f32[8]{0:T(128)S(1)} %add_rsqrt_fusion), kind=kOutput, calls=%fused_computation.29 | convolution fusion | flops 46362624 | bytes 5890080 | tf_op jit(solution)/shard_map/dot_general | solution.py:27
  194.2 19.0 %psum.111 = f32[8,1024]{1,0:T(8,128)S(1)} all-reduce(f32[8,1024]{1,0:T(8,128)S(1)} %fusion.10), channel_id=1, replica_groups=mesh['grp'=2,'kv'=4,'tp'=4] {'kv'}, use_global_device_ids=true, to_apply=%region_22.23 | all-reduce | flops 8192 | bytes 65536 | tf_op jit(solution)/shard_map/psum | solution.py:28
  213.2 0.6 fusion.23
  (14 shorter events, 0.1 us)
Async XLA Ops:
  6.5 66.3 %copy-start = (bf16[1024,1024]{1,0:T(8,128)(2,1)S(1)}, bf16[1024,1024]{1,0:T(8,128)(2,1)}, u32[]{:S(2)}) copy-start(bf16[1024,1024]{1,0:T(8,128)(2,1)} %param.26) | copy-start | bytes 6291460
  6.5 6.0 %copy-start.4 = (bf16[8,1024]{1,0:T(8,128)(2,1)S(1)}, bf16[8,1024]{1,0:T(8,128)(2,1)}, u32[]{:S(2)}) copy-start(bf16[8,1024]{1,0:T(8,128)(2,1)} %param.19) | copy-start | bytes 49156
  6.5 6.0 %copy-start.9 = (f32[1024]{0:T(1024)S(1)}, f32[1024]{0:T(1024)}, u32[]{:S(2)}) copy-start(f32[1024]{0:T(1024)} %param.20) | copy-start | bytes 12292
  6.5 41.5 %all-reduce.11.cloned.1.call-start = ((), (), s32[]{:S(2)}) async-start(), calls=%async_computation.2 | async-start | bytes 181248 | tf_op jit(solution)/shard_map/psum | solution.py:22
  6.5 6.0 %copy-start.1 = (bf16[1024,2816]{1,0:T(8,128)(2,1)S(1)}, bf16[1024,2816]{1,0:T(8,128)(2,1)}, u32[]{:S(2)}) copy-start(bf16[1024,2816]{1,0:T(8,128)(2,1)} %param.22) | copy-start | bytes 17301508
  14.0 58.1 %copy-start.5 = (f32[1024]{0:T(1024)S(1)}, f32[1024]{0:T(1024)}, u32[]{:S(2)}) copy-start(f32[1024]{0:T(1024)} %param.24) | copy-start | bytes 12292
  14.0 58.1 %copy-start.7 = (bf16[1024,32]{0,1:T(8,128)(2,1)S(1)}, bf16[1024,32]{0,1:T(8,128)(2,1)}, u32[]{:S(2)}) copy-start(bf16[1024,32]{0,1:T(8,128)(2,1)} %param.28) | copy-start | bytes 196612
  14.1 91.8 %all-reduce.7.cloned.1.call-start = ((), (), s32[]{:S(2)}) async-start(), calls=%async_computation | async-start | bytes 205824 | tf_op jit(solution)/shard_map/psum | solution.py:64
  52.3 25.2 %copy-start.11 = (s32[8]{0:T(128)S(1)}, s32[8]{0:T(128)}, u32[]{:S(2)}) copy-start(s32[8]{0:T(128)} %param.32) | copy-start | bytes 100
  71.4 5.0 %copy-start.3 = (bf16[1024,1024]{1,0:T(8,128)(2,1)S(1)}, bf16[1024,1024]{1,0:T(8,128)(2,1)}, u32[]{:S(2)}) copy-start(bf16[1024,1024]{1,0:T(8,128)(2,1)} %param.25) | copy-start | bytes 6291460
  77.5 112.5 %all-reduce.9.cloned.1.call-start = ((), (), s32[]{:S(2)}) async-start(), calls=%async_computation.1 | async-start | bytes 181248 | tf_op jit(solution)/shard_map/psum | solution.py:22
  84.0 28.0 %copy-start.6 = (f32[8,8,256]{2,1,0:T(8,128)S(1)}, f32[8,8,256]{2,1,0:T(8,128)}, u32[]{:S(2)}) copy-start(f32[8,8,256]{2,1,0:T(8,128)} %param.31) | copy-start | bytes 196612
  109.1 22.5 %copy-start.8 = (f32[8,1024]{1,0:T(8,128)S(1)}, f32[8,1024]{1,0:T(8,128)}, u32[]{:S(2)}) copy-start(f32[8,1024]{1,0:T(8,128)} %get-tuple-element.9) | copy-start | bytes 98308
  112.0 40.1 %copy-start.10 = (f32[1024]{0:T(1024)S(1)}, f32[1024]{0:T(1024)}, u32[]{:S(2)}) copy-start(f32[1024]{0:T(1024)} %param.34) | copy-start | bytes 12292
  123.2 8.4 %copy-start.2 = (bf16[1024,1024]{1,0:T(8,128)(2,1)S(1)}, bf16[1024,1024]{1,0:T(8,128)(2,1)}, u32[]{:S(2)}) copy-start(bf16[1024,1024]{1,0:T(8,128)(2,1)} %param.33) | copy-start | bytes 6291460
Sparse Core Ops, SparseCore 0:
  14.2 33.8 all-reduce.10
  77.6 28.2 all-reduce.6
  160.4 29.4 all-reduce.8
where the time goes:
time: 221 us; the launch traced here: 220 us
  waiting for transfers between devices  85.4 us (39%)
  blocking collectives  73.4 us (33%)
  matrix products  32.9 us (15%)
  between operations  13.3 us (6%)
  other arithmetic  8.63 us (4%)
  local copies, waits for them, and re-layouts  6.69 us (3%)
    psum x2, waiting for transfers between devices, half_step(): lax.psum(up_part.astype(jnp.bfloat16), 'tp').astype(jnp.float32)  63.5 us
    psum x2, blocking collectives, half_step(): down_sum = lax.psum(down_part, 'kv')  38.1 us
    psum x1, waiting for transfers between devices, attention(): lax.psum((query_part, key_part, value_part, forget_part, squares), 'tp')  21.8 us
    psum x1, blocking collectives, on_device(): lax.psum(jnp.dot(attended, out_w, preferred_element_type=jnp.float32), 'kv')  19.3 us
    dot_general x2, matrix products, half_step(): gate_part = jnp.dot(weighted, w_gate, preferred_element_type=jnp.float32)  8.61 us
    dot_general x2, matrix products, half_step(): down_part = jnp.dot(hidden, w_down, preferred_element_type=jnp.float32)  7.18 us
    reshape x1, local copies, waits for them, and re-layouts, attention(): key_block = key_cache.reshape(batch_rows, cache_span, heads_here, HEAD_DIM)  6.44 us
    dot_general x2, matrix products, half_step(): up_part = jnp.dot(weighted, w_up, preferred_element_type=jnp.float32)  5.58 us
  transfers between devices with their start and end apart: 3, of which 3 were waited for; matrix products, arithmetic and copies ran while one was open for 3% of the time, Pallas kernels for 0%

commit v1 on v0

v1 whole, which is shorter than its diff:
```python
import functools

import jax
import jax.numpy as jnp
from jax import lax
from jax.experimental import pallas as pl
from jax.experimental.pallas import tpu as pltpu
from jax.sharding import PartitionSpec as P

HEAD_DIM = 128
EPSILON = 1e-06
MASKED = -1e30
LANES = 128
MESH = pl.DeviceIdType.MESH
F32 = jnp.float32
BF16 = jnp.bfloat16


def chunk_width(columns, wanted=256):
    return wanted if columns % wanted == 0 else columns


def dot(a, b):
    return jnp.dot(a, b, preferred_element_type=F32)


class Exchange:
    def __init__(self, axis, count, buffer, send, recv, base):
        self.axis, self.count, self.buffer = axis, count, buffer
        self.send, self.recv, self.base = send, recv, base
        self.me = lax.axis_index(axis)

    def copy(self, step, window, out):
        me = self.me
        peer = lax.rem(me + step, self.count)
        origin = me if out else lax.rem(me + self.count - step, self.count)
        view = self.buffer.at[origin]
        if window is not None:
            view = view.at[:, pl.ds(*window)]
        slot = self.base + step - 1
        return pltpu.make_async_remote_copy(
            src_ref=view,
            dst_ref=view,
            send_sem=self.send.at[slot],
            recv_sem=self.recv.at[slot],
            device_id={self.axis: peer},
            device_id_type=MESH,
        )

    def start(self, window=None):
        for step in range(1, self.count):
            self.copy(step, window, True).start()

    def wait_recv(self, window=None):
        for step in range(1, self.count):
            self.copy(step, window, False).wait_recv()

    def wait_send(self, window=None):
        for step in range(1, self.count):
            self.copy(step, window, True).wait_send()


def body(n_tp, n_kv, dims, *refs):
    (
        tok_h, g1_h, wg1_h, wu1_h, wd1_h, g2_h, wq_h, wk_h, wv_h, wf_h, kc_h, vc_h, gc_h,
        len_s, wo_h, g3_h, wg2_h, wu2_h, wd2_h,
        out_ref,
        tok, g1, wg1, wu1, wd1, g2, wq, wk, wv, wf, kc, vc, gc, wo, g3, wg2, wu2, wd2,
        hid, osum, stats,
        x1a, x1b, xs1, xs2, xs3, xq, xkv, xo, xd1, xd2, xd3, xs4,
        local_sem, tp_send, tp_recv, kv_send, kv_recv,
    ) = refs
    batch, model, width, hidden, span, heads, d_full = dims
    me_tp = lax.axis_index("tp")
    me_kv = lax.axis_index("kv")

    barrier = pltpu.get_barrier_semaphore()
    for step in range(1, n_tp):
        pl.semaphore_signal(
            barrier, inc=1, device_id={"tp": lax.rem(me_tp + step, n_tp)}, device_id_type=MESH
        )
    for step in range(1, n_kv):
        pl.semaphore_signal(
            barrier, inc=1, device_id={"kv": lax.rem(me_kv + step, n_kv)}, device_id_type=MESH
        )

    used = [0]

    def load(source, target):
        copy = pltpu.make_async_copy(source, target, local_sem.at[used[0]])
        used[0] += 1
        copy.start()
        return copy

    def load_rows(source, target, pieces):
        rows = source.shape[0]
        if rows % pieces or (rows // pieces) % 16:
            pieces = 1
        size = rows // pieces
        return [
            load(source.at[pl.ds(i * size, size)], target.at[pl.ds(i * size, size)])
            for i in range(pieces)
        ]

    cw = chunk_width(hidden)
    n_chunks = hidden // cw

    def load_pair(wg_h, wu_h, wg, wu, c):
        cols = pl.ds(c * cw, cw)
        return [load(wg_h.at[:, cols], wg.at[:, cols]), load(wu_h.at[:, cols], wu.at[:, cols])]

    first_loads = [load(tok_h, tok), load(g1_h, g1)]
    pair1 = [load_pair(wg1_h, wu1_h, wg1, wu1, c) for c in range(n_chunks)]
    down1_loads = load_rows(wd1_h, wd1, 4)
    mix_loads = [load(g2_h, g2), load(wf_h, wf)]
    q_loads = load_rows(wq_h, wq, 2)
    k_loads = load_rows(wk_h, wk, 2)
    v_loads = load_rows(wv_h, wv, 2)
    key_loads = [load(gc_h, gc)] + load_rows(kc_h, kc, 1)
    val_loads = load_rows(vc_h, vc, 1)
    out_loads = load_rows(wo_h, wo, 2) + [load(g3_h, g3)]
    pair2 = [load_rows(wg2_h, wg2, 4) + load_rows(wu2_h, wu2, 4)] + [[]] * (n_chunks - 1)
    down2_loads = load_rows(wd2_h, wd2, 4)

    def wait_all(copies):
        for copy in copies:
            copy.wait()

    base_tp, base_kv = [0], [0]
    pending = []

    def tp_exchange(buffer):
        ex = Exchange("tp", n_tp, buffer, tp_send, tp_recv, base_tp[0])
        base_tp[0] += n_tp - 1
        return ex

    def kv_exchange(buffer):
        ex = Exchange("kv", n_kv, buffer, kv_send, kv_recv, base_kv[0])
        base_kv[0] += n_kv - 1
        return ex

    def begin(ex, window=None):
        ex.start(window)
        pending.append((ex, window))

    def total(buffer, count, rows=slice(None)):
        acc = buffer[0, rows].astype(F32)
        for j in range(1, count):
            acc = acc + buffer[j, rows].astype(F32)
        return acc

    lane = lax.broadcasted_iota(jnp.int32, (batch, LANES), 1)

    def half_step(rows, gain, pairs, wg, wu, down_loads, wd, x1, xs, xd, first):
        squares = jnp.sum(rows * rows, axis=1, keepdims=True)
        weighted = (rows * gain[...]).astype(BF16)
        xs[me_tp] = jnp.broadcast_to(squares, (batch, LANES))
        sq_ex = tp_exchange(xs)
        if first:
            pl.semaphore_wait(barrier, n_tp - 1 + n_kv - 1)
        begin(sq_ex)
        cut = (n_chunks + 1) // 2
        windows = []
        for lo, hi in ((0, cut), (cut, n_chunks)):
            if hi == lo:
                continue
            for c in range(lo, hi):
                wait_all(pairs[c])
                cols = pl.ds(c * cw, cw)
                both = jnp.concatenate([dot(weighted, wg[:, cols]), dot(weighted, wu[:, cols])], axis=0)
                x1[me_tp, :, cols] = both.astype(BF16)
            window = None if n_chunks == 1 else (lo * cw, (hi - lo) * cw)
            ex = tp_exchange(x1)
            begin(ex, window)
            windows.append((ex, window, slice(lo * cw, hi * cw)))
        sq_ex.wait_recv()
        scale = lax.rsqrt(total(xs, n_tp)[:, 0:1] / d_full + EPSILON)
        for ex, window, cols in windows:
            ex.wait_recv(window)
            acc = x1[0, :, cols].astype(F32)
            for j in range(1, n_tp):
                acc = acc + x1[j, :, cols].astype(F32)
            gate, up = scale * acc[:batch], scale * acc[batch:]
            hid[:, cols] = (gate / (1.0 + jnp.exp(-gate)) * up).astype(BF16)
        wait_all(down_loads)
        xd[me_kv] = dot(hid[...], wd[...]).astype(BF16)
        down_ex = kv_exchange(xd)
        begin(down_ex)
        down_ex.wait_recv()
        return (rows + 0.5 * total(xd, n_kv)).astype(BF16).astype(F32)

    wait_all(first_loads)
    after_first = half_step(
        tok[...].astype(F32), g1, pair1, wg1, wu1, down1_loads, wd1, x1a, xs1, xd1, True
    )

    squares = jnp.sum(after_first * after_first, axis=1, keepdims=True)
    wait_all(mix_loads)
    weighted = (after_first * g2[...]).astype(BF16)
    n_heads_all = wf.shape[1]
    forget = dot(weighted, wf[...])
    forget = jnp.concatenate([forget, jnp.zeros((batch, LANES - n_heads_all), F32)], axis=1)
    xs2[me_tp] = jnp.where(lane == LANES - 1, squares, forget)
    s_ex = tp_exchange(xs2)
    begin(s_ex)
    wait_all(q_loads)
    xq[me_tp] = dot(weighted, wq[...])
    q_ex = tp_exchange(xq)
    begin(q_ex)
    wait_all(k_loads)
    key_part = dot(weighted, wk[...])
    wait_all(v_loads)
    xkv[me_tp] = jnp.concatenate([key_part, dot(weighted, wv[...])], axis=0).astype(BF16)
    kv_ex = tp_exchange(xkv)
    begin(kv_ex)

    s_ex.wait_recv()
    small = total(xs2, n_tp)
    scale = lax.rsqrt(small[:, LANES - 1 :] / d_full + EPSILON)
    logits = scale * small
    log_all = jnp.minimum(logits, 0.0) - jnp.log(1.0 + jnp.exp(-jnp.abs(logits)))
    log_forget = log_all
    for k in range(1, n_kv):
        log_forget = jnp.where(
            me_kv == k, pltpu.roll(log_all, LANES - k * heads, 1), log_forget
        )
    q_ex.wait_recv()
    query = (scale * total(xq, n_tp)).astype(BF16).astype(F32)

    wait_all(key_loads)
    wait_all(val_loads)
    row_head = lax.broadcasted_iota(jnp.int32, (heads, width), 0)
    own_cols = row_head == lax.broadcasted_iota(jnp.int32, (heads, width), 1) // HEAD_DIM
    slots = me_tp * span + lax.broadcasted_iota(jnp.int32, (heads, span), 1)
    stat_row = lax.broadcasted_iota(jnp.int32, (heads, LANES), 0)
    stat_lane = lax.broadcasted_iota(jnp.int32, (heads, LANES), 1)
    half = LANES // 2
    for b in range(batch):
        spread = jnp.where(own_cols, query[b : b + 1, :], 0.0).astype(BF16)
        scores = lax.dot_general(
            spread, kc[b], (((1,), (1,)), ((), ())), preferred_element_type=F32
        ) * HEAD_DIM ** (-0.5)
        scores = scores + gc[b]
        live = slots < len_s[b]
        top = jnp.max(jnp.where(live, scores, MASKED), axis=1, keepdims=True)
        probs = jnp.where(live, jnp.exp(scores - top), 0.0)
        mass = jnp.sum(probs, axis=1, keepdims=True)
        mixed = dot(probs.astype(BF16), vc[b])
        osum[b : b + 1, :] = jnp.sum(jnp.where(own_cols, mixed, 0.0), axis=0, keepdims=True)
        placed = jnp.where(
            stat_row == stat_lane, top, jnp.where(stat_row + half == stat_lane, mass, 0.0)
        )
        stats[b : b + 1, :] = jnp.sum(placed, axis=0, keepdims=True)
    xs3[me_tp] = stats[...]
    st_ex = tp_exchange(xs3)
    begin(st_ex)
    xo[me_tp] = osum[...].astype(BF16)
    o_ex = tp_exchange(xo)
    begin(o_ex)

    kv_ex.wait_recv()
    kv_sum = total(xkv, n_tp)
    key_new = (scale * kv_sum[:batch]).astype(BF16).astype(F32)
    value_new = (scale * kv_sum[batch:]).astype(BF16).astype(F32)
    own = jnp.zeros((batch, LANES), F32)
    for h in range(heads):
        cols = slice(h * HEAD_DIM, (h + 1) * HEAD_DIM)
        own = jnp.where(
            lane == h, jnp.sum(query[:, cols] * key_new[:, cols], axis=1, keepdims=True), own
        )
    own = own * HEAD_DIM ** (-0.5)

    st_ex.wait_recv()
    tops = [xs3[j] + log_forget for j in range(n_tp)]
    highest = own
    for t in tops:
        highest = jnp.maximum(highest, t)
    factors = [jnp.exp(t - highest) for t in tops]
    own_factor = jnp.exp(own - highest)
    denom = own_factor
    for j in range(n_tp):
        denom = denom + factors[j] * pltpu.roll(xs3[j], half, 1)
    own_factor = own_factor / denom
    factors = [f / denom for f in factors]
    o_ex.wait_recv()
    pieces = []
    for h in range(heads):
        cols = slice(h * HEAD_DIM, (h + 1) * HEAD_DIM)
        acc = own_factor[:, h : h + 1] * value_new[:, cols]
        for j in range(n_tp):
            acc = acc + factors[j][:, h : h + 1] * xo[j, :, cols].astype(F32)
        pieces.append(acc.astype(BF16))
    attended = jnp.concatenate(pieces, axis=1)
    wait_all(out_loads)
    xd2[me_kv] = dot(attended, wo[...]).astype(BF16)
    p_ex = kv_exchange(xd2)
    begin(p_ex)
    p_ex.wait_recv()
    residual_two = (after_first + total(xd2, n_kv)).astype(BF16).astype(F32)

    result = half_step(
        residual_two, g3, pair2, wg2, wu2, down2_loads, wd2, x1b, xs4, xd3, False
    )
    out_ref[...] = result.astype(out_ref.dtype)
    for ex, window in pending:
        ex.wait_send(window)


def on_device(n_tp, n_kv, *args):
    (tokens, pre_gain, gate_first, up_first, down_first, mix_gain, query_w, key_w, value_w,
     forget_w, key_cache, value_cache, gate_cache, lengths, out_w, post_gain, gate_second,
     up_second, down_second) = args
    batch, model = tokens.shape
    hidden = gate_first.shape[1]
    width = query_w.shape[1]
    span = key_cache.shape[1]
    heads = width // HEAD_DIM
    d_full = model * n_tp
    row = lambda v: v.reshape(1, v.shape[0])
    operands = [tokens, row(pre_gain), gate_first, up_first, down_first, row(mix_gain), query_w,
                key_w, value_w, forget_w, key_cache, value_cache, gate_cache, lengths, out_w,
                row(post_gain), gate_second, up_second, down_second]
    lengths_at = 13
    any_spec = pl.BlockSpec(memory_space=pl.ANY)
    in_specs = [any_spec] * len(operands)
    in_specs[lengths_at] = pl.BlockSpec(memory_space=pltpu.SMEM)
    held = [pltpu.VMEM(a.shape, a.dtype) for i, a in enumerate(operands) if i != lengths_at]
    dims = (batch, model, width, hidden, span, heads, d_full)
    small = pltpu.VMEM((n_tp, batch, LANES), F32)
    cw = chunk_width(hidden)
    n_local = 2 * (hidden // cw) + 64
    tp_slots = 11 * (n_tp - 1)
    kv_slots = 3 * (n_kv - 1)
    scratch = held + [
        pltpu.VMEM((batch, hidden), BF16),
        pltpu.VMEM((batch, width), F32),
        pltpu.VMEM((batch, LANES), F32),
        pltpu.VMEM((n_tp, 2 * batch, hidden), BF16),
        pltpu.VMEM((n_tp, 2 * batch, hidden), BF16),
        small,
        small,
        small,
        pltpu.VMEM((n_tp, batch, width), F32),
        pltpu.VMEM((n_tp, 2 * batch, width), BF16),
        pltpu.VMEM((n_tp, batch, width), BF16),
        pltpu.VMEM((n_kv, batch, model), BF16),
        pltpu.VMEM((n_kv, batch, model), BF16),
        pltpu.VMEM((n_kv, batch, model), BF16),
        small,
        pltpu.SemaphoreType.DMA((n_local,)),
        pltpu.SemaphoreType.DMA((tp_slots,)),
        pltpu.SemaphoreType.DMA((tp_slots,)),
        pltpu.SemaphoreType.DMA((kv_slots,)),
        pltpu.SemaphoreType.DMA((kv_slots,)),
    ]
    return pl.pallas_call(
        functools.partial(body, n_tp, n_kv, dims),
        out_shape=jax.ShapeDtypeStruct(tokens.shape, tokens.dtype),
        in_specs=in_specs,
        out_specs=pl.BlockSpec(memory_space=pltpu.VMEM),
        scratch_shapes=scratch,
        compiler_params=pltpu.CompilerParams(
            collective_id=0, has_side_effects=True, vmem_limit_bytes=62 * 1024 * 1024
        ),
    )(*operands)


def solution(mesh):
    placed = (
        P("grp", "tp"),
        P("tp"),
        P("tp", "kv"),
        P("tp", "kv"),
        P("kv", "tp"),
        P("tp"),
        P("tp", "kv"),
        P("tp", "kv"),
        P("tp", "kv"),
        P("tp", None),
        P("grp", "tp", "kv"),
        P("grp", "tp", "kv"),
        P("grp", "kv", "tp"),
        P("grp"),
        P("kv", "tp"),
        P("tp"),
        P("tp", "kv"),
        P("tp", "kv"),
        P("kv", "tp"),
    )
    return jax.shard_map(
        functools.partial(on_device, mesh.shape["tp"], mesh.shape["kv"]),
        mesh=mesh,
        in_specs=placed,
        out_specs=P("grp", "tp"),
        check_vma=False,
    )
```

time: 221 us -> 48.6 us (0.22)
  waiting for transfers between devices: 85.4 us -> 0 us
  blocking collectives: 73.4 us -> 0 us
  Pallas kernels: 0 us -> 45.2 us
  matrix products: 32.9 us -> 0 us
  between operations: 13.3 us -> 0.01 us
  other arithmetic: 8.63 us -> 0 us
  local copies, waits for them, and re-layouts: 6.69 us -> 2.99 us
    psum x3 -> x0, waiting for transfers between devices: 85.4 us -> none  [the longest x2 63.5 us: half_step(): lax.psum(up_part.astype(jnp.bfloat16), 'tp').astype(jnp.float32)]
    psum x3 -> x0, blocking collectives: 57.4 us -> none  [the longest x2 38.1 us: half_step(): down_sum = lax.psum(down_part, 'kv')]
    pallas_call x0 -> x1, Pallas kernels: none -> 45.2 us  [on_device(): pl.pallas_call(functools.partial(body, n_tp, n_kv, dims), out_shape=jax.S...]
    dot_general x13 -> x0, matrix products: 32.9 us -> none  [the longest x2 8.61 us: half_step(): gate_part = jnp.dot(weighted, w_gate, preferred_element_type=jnp.float32)]
    all_gather x3 -> x0, blocking collectives: 15.9 us -> none  [the longest x1 5.49 us: attention(): lax.all_gather(local_mass[None].astype(jnp.bfloat16), 'tp', axis=0, tiled...]
    reshape x1 -> x0, local copies, waits for them, and re-layouts: 6.44 us -> none  [attention(): key_block = key_cache.reshape(batch_rows, cache_span, heads_here, HEAD_DIM)]
    reduce_sum x7 -> x0, other arithmetic: 4.05 us -> none  [the longest x2 2.14 us: half_step(): squares = jnp.sum(widened * widened, axis=1)]
    unnamed x24 -> x2, local copies, waits for them, and re-layouts: 0.05 us -> 2.99 us
  transfers between devices with their start and end apart: 3 -> 0, of which waited for: 3 -> 0; matrix products, arithmetic and copies ran while one was open for 3% -> 0% of each run, Pallas kernels for 0% -> 0%
where the time goes in v1:
time: 48.6 us; the launch traced here: 48.2 us
  Pallas kernels  45.2 us (93%)
  local copies, waits for them, and re-layouts  2.99 us (6%)
    pallas_call x1, Pallas kernels, on_device(): pl.pallas_call(functools.partial(body, n_tp, n_kv, dims), out_shape=jax.S...  45.2 us
    unnamed x2, local copies, waits for them, and re-layouts  2.99 us

profile of v1, /device:TPU:0, one launch (start us, length us, event | category | flops | bytes accessed | tf_op | source)
XLA Modules:
  0.0 48.2 jit_solution(14355279448584593787)
XLA Ops:
  0.0 1.7 %copy.20.refs_9_ = bf16[1024,32]{1,0:T(8,128)(2,1)} copy(bf16[1024,32]{0,1:T(8,128)(2,1)} %param.28) | data formatting | bytes 131072 | tf_op args[9]
  1.7 45.2 %shard_map.181 = bf16[8,1024]{1,0:T(8,128)(2,1)} custom-call(bf16[8,1024]{1,0:T(8,128)(2,1)} %refs_0_.1, f32[1,1024]{1,0:T(1,128)} %bitcast.3, bf16[1024,2816]{1,0:T(8,128)(2,1)} %refs_2_.1, bf16[1024,2816]{1,0:T(8,128)(2,1)} %refs_3_.1, bf16[2816,1024]{1,0:T(8,128)(2,1)} %refs_4_.1, f32[1,1024]{1,0:T(1,128)} %bitcast.4, bf16[1024,1024]{1,0:T(8,128)(2,1)} %refs_6_.1, ...), custom_call_target="tpu_custom_call" | custom-call | tf_op jit(solution)/shard_map/pallas_call | solution.py:356
  46.9 1.3 %copy.22 = bf16[8,1024]{1,0:T(8,128)(2,1)} copy(bf16[8,1024]{1,0:T(8,128)(2,1)} %shard_map.181) | data formatting | bytes 32768

commit v2 on v1

--- a/solution.py
+++ b/solution.py
@@ -11,6 +11,8 @@
 EPSILON = 1e-06
 MASKED = -1e30
 LANES = 128
+WINDOWS = 4
+KV_WINDOWS = 2
 MESH = pl.DeviceIdType.MESH
 F32 = jnp.float32
 BF16 = jnp.bfloat16
@@ -63,11 +65,11 @@
 def body(n_tp, n_kv, dims, *refs):
     (
         tok_h, g1_h, wg1_h, wu1_h, wd1_h, g2_h, wq_h, wk_h, wv_h, wf_h, kc_h, vc_h, gc_h,
-        len_s, wo_h, g3_h, wg2_h, wu2_h, wd2_h,
+        len_h, wo_h, g3_h, wg2_h, wu2_h, wd2_h,
         out_ref,
         tok, g1, wg1, wu1, wd1, g2, wq, wk, wv, wf, kc, vc, gc, wo, g3, wg2, wu2, wd2,
-        hid, osum, stats,
-        x1a, x1b, xs1, xs2, xs3, xq, xkv, xo, xd1, xd2, xd3, xs4,
+        hid, osum,
+        x1a, x1b, xs1, xs2, xs3, xq, xkv, xo, xd1, xd2, xd3, xs4, lens,
         local_sem, tp_send, tp_recv, kv_send, kv_recv,
     ) = refs
     batch, model, width, hidden, span, heads, d_full = dims
@@ -116,7 +118,7 @@
     q_loads = load_rows(wq_h, wq, 2)
     k_loads = load_rows(wk_h, wk, 2)
     v_loads = load_rows(wv_h, wv, 2)
-    key_loads = [load(gc_h, gc)] + load_rows(kc_h, kc, 1)
+    key_loads = [load(gc_h, gc), load(len_h, lens)] + load_rows(kc_h, kc, 1)
     val_loads = load_rows(vc_h, vc, 1)
     out_loads = load_rows(wo_h, wo, 2) + [load(g3_h, g3)]
     pair2 = [load_rows(wg2_h, wg2, 4) + load_rows(wu2_h, wu2, 4)] + [[]] * (n_chunks - 1)
@@ -150,6 +152,25 @@
         return acc
 
     lane = lax.broadcasted_iota(jnp.int32, (batch, LANES), 1)
+
+    def kv_product(lhs, weight, xd):
+        parts = KV_WINDOWS if model % (KV_WINDOWS * 256) == 0 else 1
+        size = model // parts
+        sent = []
+        for i in range(parts):
+            cols = slice(i * size, (i + 1) * size)
+            xd[me_kv, :, cols] = dot(lhs, weight[:, cols]).astype(BF16)
+            ex = kv_exchange(xd)
+            window = None if parts == 1 else (i * size, size)
+            begin(ex, window)
+            sent.append((ex, window, cols))
+        sums = []
+        for ex, window, cols in sent:
+            ex.wait_recv(window)
+            sums.append(xd[0, :, cols].astype(F32))
+            for j in range(1, n_kv):
+                sums[-1] = sums[-1] + xd[j, :, cols].astype(F32)
+        return jnp.concatenate(sums, axis=1)
 
     def half_step(rows, gain, pairs, wg, wu, down_loads, wd, x1, xs, xd, first):
         squares = jnp.sum(rows * rows, axis=1, keepdims=True)
@@ -159,11 +180,9 @@
         if first:
             pl.semaphore_wait(barrier, n_tp - 1 + n_kv - 1)
         begin(sq_ex)
-        cut = (n_chunks + 1) // 2
+        cuts = sorted({n_chunks * i // WINDOWS for i in range(WINDOWS + 1)})
         windows = []
-        for lo, hi in ((0, cut), (cut, n_chunks)):
-            if hi == lo:
-                continue
+        for lo, hi in zip(cuts[:-1], cuts[1:]):
             for c in range(lo, hi):
                 wait_all(pairs[c])
                 cols = pl.ds(c * cw, cw)
@@ -183,11 +202,7 @@
             gate, up = scale * acc[:batch], scale * acc[batch:]
             hid[:, cols] = (gate / (1.0 + jnp.exp(-gate)) * up).astype(BF16)
         wait_all(down_loads)
-        xd[me_kv] = dot(hid[...], wd[...]).astype(BF16)
-        down_ex = kv_exchange(xd)
-        begin(down_ex)
-        down_ex.wait_recv()
-        return (rows + 0.5 * total(xd, n_kv)).astype(BF16).astype(F32)
+        return (rows + 0.5 * kv_product(hid[...], wd, xd)).astype(BF16).astype(F32)
 
     wait_all(first_loads)
     after_first = half_step(
@@ -197,8 +212,10 @@
     squares = jnp.sum(after_first * after_first, axis=1, keepdims=True)
     wait_all(mix_loads)
     weighted = (after_first * g2[...]).astype(BF16)
-    n_heads_all = wf.shape[1]
-    forget = dot(weighted, wf[...])
+    n_heads_all = wf.shape[0]
+    forget = lax.dot_general(
+        weighted, wf[...], (((1,), (1,)), ((), ())), preferred_element_type=F32
+    )
     forget = jnp.concatenate([forget, jnp.zeros((batch, LANES - n_heads_all), F32)], axis=1)
     xs2[me_tp] = jnp.where(lane == LANES - 1, squares, forget)
     s_ex = tp_exchange(xs2)
@@ -235,25 +252,29 @@
     stat_row = lax.broadcasted_iota(jnp.int32, (heads, LANES), 0)
     stat_lane = lax.broadcasted_iota(jnp.int32, (heads, LANES), 1)
     half = LANES // 2
+    all_scores = []
     for b in range(batch):
         spread = jnp.where(own_cols, query[b : b + 1, :], 0.0).astype(BF16)
-        scores = lax.dot_general(
-            spread, kc[b], (((1,), (1,)), ((), ())), preferred_element_type=F32
-        ) * HEAD_DIM ** (-0.5)
-        scores = scores + gc[b]
-        live = slots < len_s[b]
+        all_scores.append(
+            lax.dot_general(spread, kc[b], (((1,), (1,)), ((), ())), preferred_element_type=F32)
+        )
+    all_probs = []
+    for b in range(batch):
+        scores = all_scores[b] * HEAD_DIM ** (-0.5) + gc[b]
+        live = slots < lens[b]
         top = jnp.max(jnp.where(live, scores, MASKED), axis=1, keepdims=True)
         probs = jnp.where(live, jnp.exp(scores - top), 0.0)
         mass = jnp.sum(probs, axis=1, keepdims=True)
-        mixed = dot(probs.astype(BF16), vc[b])
-        osum[b : b + 1, :] = jnp.sum(jnp.where(own_cols, mixed, 0.0), axis=0, keepdims=True)
+        all_probs.append(probs.astype(BF16))
         placed = jnp.where(
             stat_row == stat_lane, top, jnp.where(stat_row + half == stat_lane, mass, 0.0)
         )
-        stats[b : b + 1, :] = jnp.sum(placed, axis=0, keepdims=True)
-    xs3[me_tp] = stats[...]
+        xs3[me_tp, b : b + 1, :] = jnp.sum(placed, axis=0, keepdims=True)
     st_ex = tp_exchange(xs3)
     begin(st_ex)
+    for b in range(batch):
+        mixed = dot(all_probs[b], vc[b])
+        osum[b : b + 1, :] = jnp.sum(jnp.where(own_cols, mixed, 0.0), axis=0, keepdims=True)
     xo[me_tp] = osum[...].astype(BF16)
     o_ex = tp_exchange(xo)
     begin(o_ex)
@@ -292,11 +313,7 @@
         pieces.append(acc.astype(BF16))
     attended = jnp.concatenate(pieces, axis=1)
     wait_all(out_loads)
-    xd2[me_kv] = dot(attended, wo[...]).astype(BF16)
-    p_ex = kv_exchange(xd2)
-    begin(p_ex)
-    p_ex.wait_recv()
-    residual_two = (after_first + total(xd2, n_kv)).astype(BF16).astype(F32)
+    residual_two = (after_first + kv_product(attended, wo, xd2)).astype(BF16).astype(F32)
 
     result = half_step(
         residual_two, g3, pair2, wg2, wu2, down2_loads, wd2, x1b, xs4, xd3, False
@@ -318,23 +335,21 @@
     d_full = model * n_tp
     row = lambda v: v.reshape(1, v.shape[0])
     operands = [tokens, row(pre_gain), gate_first, up_first, down_first, row(mix_gain), query_w,
-                key_w, value_w, forget_w, key_cache, value_cache, gate_cache, lengths, out_w,
+                key_w, value_w, forget_w.T, key_cache, value_cache, gate_cache, lengths, out_w,
                 row(post_gain), gate_second, up_second, down_second]
     lengths_at = 13
     any_spec = pl.BlockSpec(memory_space=pl.ANY)
     in_specs = [any_spec] * len(operands)
-    in_specs[lengths_at] = pl.BlockSpec(memory_space=pltpu.SMEM)
     held = [pltpu.VMEM(a.shape, a.dtype) for i, a in enumerate(operands) if i != lengths_at]
     dims = (batch, model, width, hidden, span, heads, d_full)
     small = pltpu.VMEM((n_tp, batch, LANES), F32)
     cw = chunk_width(hidden)
     n_local = 2 * (hidden // cw) + 64
-    tp_slots = 11 * (n_tp - 1)
-    kv_slots = 3 * (n_kv - 1)
+    tp_slots = (7 + 2 * WINDOWS) * (n_tp - 1)
+    kv_slots = 3 * KV_WINDOWS * (n_kv - 1)
     scratch = held + [
         pltpu.VMEM((batch, hidden), BF16),
         pltpu.VMEM((batch, width), F32),
-        pltpu.VMEM((batch, LANES), F32),
         pltpu.VMEM((n_tp, 2 * batch, hidden), BF16),
         pltpu.VMEM((n_tp, 2 * batch, hidden), BF16),
         small,
@@ -347,6 +362,7 @@
         pltpu.VMEM((n_kv, batch, model), BF16),
         pltpu.VMEM((n_kv, batch, model), BF16),
         small,
+        pltpu.SMEM((lengths.shape[0],), lengths.dtype),
         pltpu.SemaphoreType.DMA((n_local,)),
         pltpu.SemaphoreType.DMA((tp_slots,)),
         pltpu.SemaphoreType.DMA((tp_slots,)),

time: 48.6 us -> 42.6 us (0.88)
  Pallas kernels: 45.2 us -> 41 us
  local copies, waits for them, and re-layouts: 2.99 us -> 1.32 us
    pallas_call x1, Pallas kernels: 45.2 us -> 41 us  [on_device(): pl.pallas_call(functools.partial(body, n_tp, n_kv, dims), out_shape=jax.S...]
    unnamed x2 -> x1, local copies, waits for them, and re-layouts: 2.99 us -> 1.32 us
where the time goes in v2:
time: 42.6 us; the launch traced here: 42.3 us
  Pallas kernels  41 us (96%)
  local copies, waits for them, and re-layouts  1.32 us (3%)
    pallas_call x1, Pallas kernels, on_device(): pl.pallas_call(functools.partial(body, n_tp, n_kv, dims), out_shape=jax.S...  41 us
    unnamed x1, local copies, waits for them, and re-layouts  1.32 us

profile of v2, /device:TPU:0, one launch (start us, length us, event | category | flops | bytes accessed | tf_op | source)
XLA Modules:
  0.0 42.3 jit_solution(11047787736084436591)
XLA Ops:
  0.0 41.0 %shard_map.181 = bf16[8,1024]{1,0:T(8,128)(2,1)} custom-call(bf16[8,1024]{1,0:T(8,128)(2,1)} %refs_0_.1, f32[1,1024]{1,0:T(1,128)} %bitcast.5, bf16[1024,2816]{1,0:T(8,128)(2,1)} %refs_2_.1, bf16[1024,2816]{1,0:T(8,128)(2,1)} %refs_3_.1, bf16[2816,1024]{1,0:T(8,128)(2,1)} %refs_4_.1, f32[1,1024]{1,0:T(1,128)} %bitcast.6, bf16[1024,1024]{1,0:T(8,128)(2,1)} %refs_6_.1, ...), custom_call_target="tpu_custom_call" | custom-call | tf_op jit(solution)/shard_map/pallas_call | solution.py:372
  41.0 1.3 %copy.21 = bf16[8,1024]{1,0:T(8,128)(2,1)} copy(bf16[8,1024]{1,0:T(8,128)(2,1)} %shard_map.181) | data formatting | bytes 32768
